TPU v7x, 32 devices: a whole 2x2x4 slice. The times are simulated.
32 devices in a mesh: fs: 8 (over z, y), tp: 4 (over x, core).
Axes of the slice: x: 2, y: 2, z: 4, core: 2. Of those that a mesh axis runs over, the one named last changes fastest.
Arguments:
- tokens: bfloat16 [8192, 2048], P('fs', 'tp'), may hold values from -6 to 6
- norm_gain: float32 [2048], P('fs'), may hold values from 0.1 to 1.9
- up_master: float32 [2048, 4096], P('fs', 'tp'), may hold values from -0.125 to 0.125
- down_master: float32 [4096, 2048], P('fs', 'tp'), may hold values from -0.09375 to 0.09375
Outputs:
- mixed: bfloat16 [8192, 2048], P('fs', 'tp')
- up_ready: bfloat16 [2048, 4096], P(None, 'tp')
- down_ready: bfloat16 [4096, 2048], P('tp')
All inputs are finite; a program needn't handle non-finite values.
Results may differ from a plain program's by a relative error of at most 0.0095.
Values may be sent and summed in bfloat16 or wider, within the bound.
A program may use at most 128 MiB of HBM per device.

v0:
```python
import jax
import jax.numpy as jnp
from jax import lax
from jax.sharding import PartitionSpec as P


def shards(tokens, norm_gain, up_master, down_master):
    up_local = (norm_gain[:, None] * up_master).astype(jnp.bfloat16)
    up_ready = lax.all_gather(up_local, "fs", axis=0, tiled=True)
    down_local = down_master.astype(jnp.bfloat16)
    gathered = lax.all_gather(down_local, "fs", axis=0, tiled=True)
    down_ready = lax.all_to_all(gathered, "tp", split_axis=0, concat_axis=1, tiled=True)
    features = lax.all_gather(tokens, "tp", axis=1, tiled=True)
    values = features.astype(jnp.float32)
    mean_square = jnp.mean(values * values, axis=-1, keepdims=True)
    normed = (values * lax.rsqrt(mean_square + 1e-06)).astype(jnp.bfloat16)
    before = jnp.dot(normed, up_ready, preferred_element_type=jnp.float32)
    hidden = jnp.square(jax.nn.relu(before)).astype(jnp.bfloat16)
    partial_value = jnp.dot(hidden, down_ready, preferred_element_type=jnp.float32)
    mixed = lax.psum_scatter(
        partial_value.astype(jnp.bfloat16), "tp", scatter_dimension=1, tiled=True
    )
    return (mixed, up_ready, down_ready)


def solution(mesh):
    return jax.shard_map(
        shards,
        mesh=mesh,
        in_specs=(P("fs", "tp"), P("fs"), P("fs", "tp"), P("fs", "tp")),
        out_specs=(P("fs", "tp"), P(None, "tp"), P("tp", None)),
        check_vma=False,
    )
```

profile of v0, /device:TPU:0, one launch (start us, length us, event | category | flops | bytes accessed | tf_op | source)
XLA Modules:
  0.0 287.9 jit_solution(17428654618168584598)
XLA Ops:
  7.2 0.0 all-gather.8.cloned.1.call-start
  7.2 2.1 convert_element_type.22
  9.3 0.0 all-gather.8.cloned.1.call-update
  9.3 0.0 all-gather.4.cloned.1.call-start
  9.4 0.7 all-gather.4.cloned.1.call-update
  10.1 0.0 all-gather.6.cloned.1.call-start
  10.1 2.1 multiply_convert_fusion.2
  12.3 0.0 all-gather.6.cloned.1.call-update
  12.3 73.9 %all-gather.8.cloned.1.call-done = bf16[4096,512]{1,0:T(8,128)(2,1)} async-done(((bf16[512,512]{1,0:T(8,128)(2,1)}), bf16[4096,512]{1,0:T(8,128)(2,1)}) %all-gather.8.cloned.1.call-update) | async-done | bytes 4194320 | tf_op jit(solution)/shard_map/all_gather | solution.py:11
  86.2 4.9 %all-to-all-start = ((bf16[4,1024,512]{2,1,0:T(8,128)(2,1)}), bf16[4,1024,512]{2,1,0:T(8,128)(2,1)}, u32[]{:S(2)}, u32[]{:S(2)}) async-start(bf16[4,1024,512]{2,1,0:T(8,128)(2,1)} %bitcast.8), calls=%async_computation | async-start | bytes 8388608 | tf_op jit(solution)/shard_map/all_to_all | solution.py:12
  91.1 0.0 reduce-scatter.2.cloned.1.call-start
  91.2 52.2 %all-gather.4.cloned.1.call-done = bf16[1024,2048]{1,0:T(8,128)(2,1)} async-done(((bf16[1024,512]{1,0:T(8,128)(2,1)}), bf16[1024,2048]{1,0:T(8,128)(2,1)}) %all-gather.4.cloned.1.call-update) | async-done | bytes 4194320 | tf_op jit(solution)/shard_map/all_gather | solution.py:13
  143.4 3.1 %fusion = f32[1024]{0:T(1024)S(1)} fusion(bf16[1024,2048]{1,0:T(8,128)(2,1)} %all-gather.4.cloned.1.call-done), kind=kLoop, calls=%fused_computation.2 | loop fusion | flops 6290432 | bytes 4198400 | tf_op jit(solution)/shard_map/reduce_sum | solution.py:15
  146.5 15.3 %all-to-all-done = bf16[4,1024,512]{2,1,0:T(8,128)(2,1)} async-done(((bf16[4,1024,512]{2,1,0:T(8,128)(2,1)}), bf16[4,1024,512]{2,1,0:T(8,128)(2,1)}, u32[]{:S(2)}, u32[]{:S(2)}) %all-to-all-start) | async-done | bytes 4194336 | tf_op jit(solution)/shard_map/all_to_all | solution.py:12
  161.8 6.2 %copy.8 = bf16[4,1024,512]{1,2,0:T(8,128)(2,1)} copy(bf16[4,1024,512]{2,1,0:T(8,128)(2,1)} %all-to-all-done) | data formatting | bytes 8388608 | tf_op jit(solution)/shard_map/all_to_all | solution.py:12
  168.0 50.9 %all-gather.6.cloned.1.call-done = bf16[2048,1024]{1,0:T(8,128)(2,1)} async-done(((bf16[256,1024]{1,0:T(8,128)(2,1)}), bf16[2048,1024]{1,0:T(8,128)(2,1)}) %all-gather.6.cloned.1.call-update) | async-done | bytes 4194320 | tf_op jit(solution)/shard_map/all_gather | solution.py:9
  218.9 14.7 %convolution_convert_fusion = bf16[1024,2048]{1,0:T(8,128)(2,1)} fusion(bf16[1024,2048]{0,1:T(8,128)(2,1)} %bitcast.6, bf16[2048,1024]{1,0:T(8,128)(2,1)} %all-gather.6.cloned.1.call-done, bf16[1024,2048]{1,0:T(8,128)(2,1)} %all-gather.4.cloned.1.call-done, f32[1024]{0:T(1024)S(1)} %add_rsqrt_fusion), kind=kOutput, calls=%fused_computation.7 | convolution fusion | flops 8601468928 | bytes 16781312 | tf_op jit(solution)/shard_map/dot_general | solution.py:19
  233.6 0.0 reduce-scatter.2.cloned.1.call-update
  233.6 6.5 %copy.9 = bf16[1024,2048]{1,0:T(8,128)(2,1)} copy(bf16[1024,2048]{0,1:T(8,128)(2,1)} %bitcast.7) | data formatting | bytes 8388608
  240.1 36.6 %reduce-scatter.2.cloned.1.call-done = bf16[1024,512]{1,0:T(8,128)(2,1)} async-done(((bf16[1024,2048]{1,0:T(8,128)(2,1)}), bf16[1024,512]{1,0:T(8,128)(2,1)}) %reduce-scatter.2.cloned.1.call-update) | async-done | bytes 1048592 | tf_op jit(solution)/shard_map/reduce_scatter | solution.py:20
  276.7 4.6 %copy.11 = bf16[2048,1024]{1,0:T(8,128)(2,1)} copy(bf16[2048,1024]{1,0:T(8,128)(2,1)} %all-gather.6.cloned.1.call-done) | data formatting | bytes 8388608
  (1 shorter events, 0.0 us)
Async XLA Ops:
  7.2 79.1 %all-gather.8.cloned.1.call-start = ((), (), s32[]{:S(2)}) async-start(), calls=%async_computation.4 | async-start | bytes 4718592 | tf_op jit(solution)/shard_map/all_gather | solution.py:11
  9.3 134.1 %all-gather.4.cloned.1.call-start = ((), (), s32[]{:S(2)}) async-start(), calls=%async_computation.2 | async-start | bytes 5242880 | tf_op jit(solution)/shard_map/all_gather | solution.py:13
  10.1 208.8 %all-gather.6.cloned.1.call-start = ((), (), s32[]{:S(2)}) async-start(), calls=%async_computation.3 | async-start | bytes 4718592 | tf_op jit(solution)/shard_map/all_gather | solution.py:9
  86.2 75.6 %all-to-all-start = ((bf16[4,1024,512]{2,1,0:T(8,128)(2,1)}), bf16[4,1024,512]{2,1,0:T(8,128)(2,1)}, u32[]{:S(2)}, u32[]{:S(2)}) async-start(bf16[4,1024,512]{2,1,0:T(8,128)(2,1)} %bitcast.8), calls=%async_computation | async-start | bytes 8388608 | tf_op jit(solution)/shard_map/all_to_all | solution.py:12
  91.1 185.6 %reduce-scatter.2.cloned.1.call-start = ((), (), s32[]{:S(2)}) async-start(), calls=%async_computation.5 | async-start | bytes 5242880 | tf_op jit(solution)/shard_map/reduce_scatter | solution.py:20
Sparse Core Ops, SparseCore 0:
  10.7 75.5 all-gather.7
  87.8 55.5 all-gather.3
  146.1 72.7 all-gather.5
  233.7 42.9 reduce-scatter.1
where the time goes:
time: 288 us
  waiting for transfers between devices  230 us (80%)
  local copies, waits for them, and re-layouts  17.3 us (6%)
  matrix products  14.7 us (5%)
  between operations  13.8 us (5%)
  other arithmetic  7.31 us (3%)
  starting transfers between devices  5.06 us (2%)
    all_gather x1, waiting for transfers between devices, shards(): gathered = lax.all_gather(down_local, 'fs', axis=0, tiled=True)  73.9 us
    all_gather x1, waiting for transfers between devices, shards(): features = lax.all_gather(tokens, 'tp', axis=1, tiled=True)  52.2 us
    all_gather x1, waiting for transfers between devices, shards(): up_ready = lax.all_gather(up_local, 'fs', axis=0, tiled=True)  50.9 us
    reduce_scatter x1, waiting for transfers between devices, shards(): lax.psum_scatter(partial_value.astype(jnp.bfloat16), 'tp', scatter_dimens...  36.6 us
    all_to_all x1, waiting for transfers between devices, shards(): lax.all_to_all(gathered, 'tp', split_axis=0, concat_axis=1, tiled=True)  15.3 us
    dot_general x1, matrix products, shards(): jnp.dot(hidden, down_ready, preferred_element_type=jnp.float32)  14.7 us
    unnamed x2, local copies, waits for them, and re-layouts  11.1 us
    all_to_all x1, local copies, waits for them, and re-layouts, shards(): lax.all_to_all(gathered, 'tp', split_axis=0, concat_axis=1, tiled=True)  6.21 us
  transfers between devices with their start and end apart: 5, of which 5 were waited for; matrix products, arithmetic and copies ran while one was open for 6% of the time, Pallas kernels for 0%

commit v1 on v0

--- a/solution.py
+++ b/solution.py
@@ -4,9 +4,23 @@
 from jax.sharding import PartitionSpec as P
 
 
+def wrap_the_strings(a0):
+    sides = lax.psum(1, axis_name="fs")
+    state_next = [(k0 - 1, k0) for k0 in range(1, sides)] + [(sides - 1, 0)]
+    mixed_arr = a0
+    history = [mixed_arr]
+    for _ in range(sides - 1):
+        mixed_arr = lax.ppermute(mixed_arr, axis_name="fs", perm=state_next)
+        history += [mixed_arr]
+    o_now = jnp.concatenate([*reversed(history)], axis=0)
+    w2 = lax.axis_index("fs")
+    response = jnp.roll(o_now, shift=(w2 + 1) * mixed_arr.shape[0], axis=0)
+    return response
+
+
 def shards(tokens, norm_gain, up_master, down_master):
     up_local = (norm_gain[:, None] * up_master).astype(jnp.bfloat16)
-    up_ready = lax.all_gather(up_local, "fs", axis=0, tiled=True)
+    up_ready = wrap_the_strings(up_local)
     down_local = down_master.astype(jnp.bfloat16)
     gathered = lax.all_gather(down_local, "fs", axis=0, tiled=True)
     down_ready = lax.all_to_all(gathered, "tp", split_axis=0, concat_axis=1, tiled=True)

time: 288 us -> 276 us (0.958)
  waiting for transfers between devices: 230 us -> 210 us
  local copies, waits for them, and re-layouts: 17.3 us -> 21.7 us
  starting transfers between devices: 5.06 us -> 8.48 us
    ppermute x0 -> x7, waiting for transfers between devices: none -> 137 us  [wrap_the_strings(): mixed_arr = lax.ppermute(mixed_arr, axis_name='fs', perm=state_next)]
    all_gather x1, waiting for transfers between devices: 73.9 us -> 0.01 us  [shards(): gathered = lax.all_gather(down_local, 'fs', axis=0, tiled=True)]
    all_gather x1, waiting for transfers between devices: 52.2 us -> 0.01 us  [shards(): features = lax.all_gather(tokens, 'tp', axis=1, tiled=True)]
    all_gather x1 -> x0, waiting for transfers between devices: 50.9 us -> none  [shards(): up_ready = lax.all_gather(up_local, 'fs', axis=0, tiled=True)]
    all_to_all x1, waiting for transfers between devices: 15.3 us -> 32.5 us  [shards(): lax.all_to_all(gathered, 'tp', split_axis=0, concat_axis=1, tiled=True)]
    ppermute x0 -> x7, starting transfers between devices: none -> 3.4 us  [wrap_the_strings(): mixed_arr = lax.ppermute(mixed_arr, axis_name='fs', perm=state_next)]
    unnamed x2 -> x23, local copies, waits for them, and re-layouts: 11.1 us -> 13 us
  transfers between devices with their start and end apart: 5 -> 11, of which waited for: 5 -> 9; matrix products, arithmetic and copies ran while one was open for 6% -> 7% of each run, Pallas kernels for 0% -> 0%
where the time goes in v1:
time: 276 us; the launch traced here: 275 us
  waiting for transfers between devices  210 us (76%)
  local copies, waits for them, and re-layouts  21.7 us (8%)
  matrix products  14.7 us (5%)
  between operations  13.9 us (5%)
  starting transfers between devices  8.48 us (3%)
  other arithmetic  6.84 us (2%)
    ppermute x7, waiting for transfers between devices, wrap_the_strings(): mixed_arr = lax.ppermute(mixed_arr, axis_name='fs', perm=state_next)  137 us
    reduce_scatter x1, waiting for transfers between devices, shards(): lax.psum_scatter(partial_value.astype(jnp.bfloat16), 'tp', scatter_dimens...  39.2 us
    all_to_all x1, waiting for transfers between devices, shards(): lax.all_to_all(gathered, 'tp', split_axis=0, concat_axis=1, tiled=True)  32.5 us
    dot_general x1, matrix products, shards(): jnp.dot(hidden, down_ready, preferred_element_type=jnp.float32)  14.7 us
    unnamed x23, local copies, waits for them, and re-layouts  13 us
    all_to_all x1, local copies, waits for them, and re-layouts, shards(): lax.all_to_all(gathered, 'tp', split_axis=0, concat_axis=1, tiled=True)  6.31 us
  transfers between devices with their start and end apart: 11, of which 9 were waited for; matrix products, arithmetic and copies ran while one was open for 7% of the time, Pallas kernels for 0%

profile of v1, /device:TPU:0, one launch (start us, length us, event | category | flops | bytes accessed | tf_op | source)
XLA Modules:
  0.0 275.4 jit_solution(557496342218837508)
XLA Ops:
  7.2 0.0 all-gather.5.cloned.1.call-start
  7.2 2.1 convert_element_type.22
  9.3 0.0 all-gather.5.cloned.1.call-update
  9.3 0.0 all-gather.3.cloned.1.call-start
  9.4 0.7 all-gather.3.cloned.1.call-update
  10.1 0.0 copy-start
  10.1 0.0 copy-start.3
  10.1 1.4 multiply_convert_fusion.2
  11.5 3.0 %collective-permute-start = (bf16[256,1024]{1,0:T(8,128)(2,1)S(1)}, bf16[256,1024]{1,0:T(8,128)(2,1)S(1)}, u32[]{:S(2)}, u32[]{:S(2)}) collective-permute-start(bf16[256,1024]{1,0:T(8,128)(2,1)S(1)} %multiply_convert_fusion.2), channel_id=1, source_target_pairs={{0,4},{4,8},{8,12},{12,16},{16,20},{20,24},{24,28},{28,0},{1,5},{5... | collective-permute-start | bytes 1572872 | tf_op jit(solution)/shard_map/ppermute | solution.py:13
  14.6 18.2 %collective-permute-done = bf16[256,1024]{1,0:T(8,128)(2,1)S(1)} collective-permute-done((bf16[256,1024]{1,0:T(8,128)(2,1)S(1)}, bf16[256,1024]{1,0:T(8,128)(2,1)S(1)}, u32[]{:S(2)}, u32[]{:S(2)}) %collective-permute-start) | collective-permute-done | bytes 524320 | tf_op jit(solution)/shard_map/ppermute | solution.py:13
  32.7 0.3 collective-permute-start.1
  33.1 24.6 %collective-permute-done.1 = bf16[256,1024]{1,0:T(8,128)(2,1)S(1)} collective-permute-done((bf16[256,1024]{1,0:T(8,128)(2,1)S(1)}, bf16[256,1024]{1,0:T(8,128)(2,1)S(1)}, u32[]{:S(2)}, u32[]{:S(2)}) %collective-permute-start.1) | collective-permute-done | bytes 524320 | tf_op jit(solution)/shard_map/ppermute | solution.py:13
  57.7 0.0 collective-permute-start.2
  57.7 26.8 %collective-permute-done.2 = bf16[256,1024]{1,0:T(8,128)(2,1)S(1)} collective-permute-done((bf16[256,1024]{1,0:T(8,128)(2,1)S(1)}, bf16[256,1024]{1,0:T(8,128)(2,1)S(1)}, u32[]{:S(2)}, u32[]{:S(2)}) %collective-permute-start.2) | collective-permute-done | bytes 524320 | tf_op jit(solution)/shard_map/ppermute | solution.py:13
  84.6 0.0 collective-permute-start.3
  84.6 26.9 %collective-permute-done.3 = bf16[256,1024]{1,0:T(8,128)(2,1)S(1)} collective-permute-done((bf16[256,1024]{1,0:T(8,128)(2,1)S(1)}, bf16[256,1024]{1,0:T(8,128)(2,1)S(1)}, u32[]{:S(2)}, u32[]{:S(2)}) %collective-permute-start.3) | collective-permute-done | bytes 524320 | tf_op jit(solution)/shard_map/ppermute | solution.py:13
  111.5 0.0 collective-permute-start.4
  111.5 18.0 %collective-permute-done.4 = bf16[256,1024]{1,0:T(8,128)(2,1)S(1)} collective-permute-done((bf16[256,1024]{1,0:T(8,128)(2,1)S(1)}, bf16[256,1024]{1,0:T(8,128)(2,1)S(1)}, u32[]{:S(2)}, u32[]{:S(2)}) %collective-permute-start.4) | collective-permute-done | bytes 524320 | tf_op jit(solution)/shard_map/ppermute | solution.py:13
  129.5 0.0 copy-start.1
  129.5 0.8 copy-done.1
  130.3 0.0 collective-permute-start.5
  130.3 14.2 %collective-permute-done.5 = bf16[256,1024]{1,0:T(8,128)(2,1)} collective-permute-done((bf16[256,1024]{1,0:T(8,128)(2,1)S(1)}, bf16[256,1024]{1,0:T(8,128)(2,1)}, u32[]{:S(2)}, u32[]{:S(2)}) %collective-permute-start.5) | collective-permute-done | bytes 524320 | tf_op jit(solution)/shard_map/ppermute | solution.py:13
  144.5 0.0 collective-permute-start.6
  144.5 0.0 all-gather.5.cloned.1.call-done
  144.5 5.0 %all-to-all-start = ((bf16[4,1024,512]{2,1,0:T(8,128)(2,1)}), bf16[4,1024,512]{2,1,0:T(8,128)(2,1)}, u32[]{:S(2)}, u32[]{:S(2)}) async-start(bf16[4,1024,512]{2,1,0:T(8,128)(2,1)} %bitcast.8), calls=%async_computation | async-start | bytes 8388608 | tf_op jit(solution)/shard_map/all_to_all | solution.py:26
  149.5 0.0 reduce-scatter.2.cloned.1.call-start
  149.6 0.0 copy-start.2
  149.6 8.5 %collective-permute-done.6 = bf16[256,1024]{1,0:T(8,128)(2,1)} collective-permute-done((bf16[256,1024]{1,0:T(8,128)(2,1)}, bf16[256,1024]{1,0:T(8,128)(2,1)}, u32[]{:S(2)}, u32[]{:S(2)}) %collective-permute-start.6) | collective-permute-done | bytes 524320 | tf_op jit(solution)/shard_map/ppermute | solution.py:13
  158.1 1.1 constant_dynamic-update-slice_fusion.15
  159.2 1.1 constant_dynamic-update-slice_fusion.14
  160.3 1.1 constant_dynamic-update-slice_fusion.13
  161.5 0.0 copy-done
  161.5 0.0 copy-done.3
  161.6 0.1 constant_dynamic-update-slice_fusion.8
  161.7 1.1 constant_dynamic-update-slice_fusion.7
  162.8 1.1 constant_dynamic-update-slice_fusion.6
  163.8 0.0 copy-done.2
  164.1 0.1 constant_dynamic-update-slice_fusion
  164.2 2.5 constant_dynamic-slice_fusion
  166.7 0.0 all-gather.3.cloned.1.call-done
  166.7 3.1 %fusion = f32[1024]{0:T(1024)S(1)} fusion(bf16[1024,2048]{1,0:T(8,128)(2,1)} %all-gather.3.cloned.1.call-done), kind=kLoop, calls=%fused_computation.2 | loop fusion | flops 6290432 | bytes 4198400 | tf_op jit(solution)/shard_map/reduce_sum | solution.py:29
  169.8 32.5 %all-to-all-done = bf16[4,1024,512]{2,1,0:T(8,128)(2,1)} async-done(((bf16[4,1024,512]{2,1,0:T(8,128)(2,1)}), bf16[4,1024,512]{2,1,0:T(8,128)(2,1)}, u32[]{:S(2)}, u32[]{:S(2)}) %all-to-all-start) | async-done | bytes 4194336 | tf_op jit(solution)/shard_map/all_to_all | solution.py:26
  202.2 6.3 %copy.8 = bf16[4,1024,512]{1,2,0:T(8,128)(2,1)} copy(bf16[4,1024,512]{2,1,0:T(8,128)(2,1)} %all-to-all-done) | data formatting | bytes 8388608 | tf_op jit(solution)/shard_map/all_to_all | solution.py:26
  208.5 14.7 %convolution_convert_fusion = bf16[1024,2048]{1,0:T(8,128)(2,1)} fusion(bf16[1024,2048]{0,1:T(8,128)(2,1)} %bitcast.6, bf16[2048,1024]{1,0:T(8,128)(2,1)} %constant_dynamic-slice_fusion, bf16[1024,2048]{1,0:T(8,128)(2,1)} %all-gather.3.cloned.1.call-done, f32[1024]{0:T(1024)S(1)} %add_rsqrt_fusion), kind=kOutput, calls=%fused_computation.7 | convolution fusion | flops 8601468928 | bytes 16781312 | tf_op jit(solution)/shard_map/dot_general | solution.py:33
  223.3 0.0 reduce-scatter.2.cloned.1.call-update
  223.3 6.4 %copy.9 = bf16[1024,2048]{1,0:T(8,128)(2,1)} copy(bf16[1024,2048]{0,1:T(8,128)(2,1)} %bitcast.7) | data formatting | bytes 8388608
  229.7 39.2 %reduce-scatter.2.cloned.1.call-done = bf16[1024,512]{1,0:T(8,128)(2,1)} async-done(((bf16[1024,2048]{1,0:T(8,128)(2,1)}), bf16[1024,512]{1,0:T(8,128)(2,1)}) %reduce-scatter.2.cloned.1.call-update) | async-done | bytes 1048592 | tf_op jit(solution)/shard_map/reduce_scatter | solution.py:34
  (10 shorter events, 0.3 us)
Async XLA Ops:
  7.2 137.4 %all-gather.5.cloned.1.call-start = ((), (), s32[]{:S(2)}) async-start(), calls=%async_computation.3 | async-start | bytes 4718592 | tf_op jit(solution)/shard_map/all_gather | solution.py:25
  9.3 157.4 %all-gather.3.cloned.1.call-start = ((), (), s32[]{:S(2)}) async-start(), calls=%async_computation.2 | async-start | bytes 5242880 | tf_op jit(solution)/shard_map/all_gather | solution.py:27
  10.1 151.5 %copy-start = (f32[256,1024]{1,0:T(8,128)S(1)}, f32[256,1024]{1,0:T(8,128)}, u32[]{:S(2)}) copy-start(f32[256,1024]{1,0:T(8,128)} %param.6) | copy-start | bytes 3145732
  10.1 151.5 %copy-start.3 = (f32[256]{0:T(256)S(1)}, f32[256]{0:T(256)}, u32[]{:S(2)}) copy-start(f32[256]{0:T(256)} %param.5) | copy-start | bytes 3076
  11.5 21.2 %collective-permute-start = (bf16[256,1024]{1,0:T(8,128)(2,1)S(1)}, bf16[256,1024]{1,0:T(8,128)(2,1)S(1)}, u32[]{:S(2)}, u32[]{:S(2)}) collective-permute-start(bf16[256,1024]{1,0:T(8,128)(2,1)S(1)} %multiply_convert_fusion.2), channel_id=1, source_target_pairs={{0,4},{4,8},{8,12},{12,16},{16,20},{20,24},{24,28},{28,0},{1,5},{5... | collective-permute-start | bytes 1572872 | tf_op jit(solution)/shard_map/ppermute | solution.py:13
  32.7 25.0 %collective-permute-start.1 = (bf16[256,1024]{1,0:T(8,128)(2,1)S(1)}, bf16[256,1024]{1,0:T(8,128)(2,1)S(1)}, u32[]{:S(2)}, u32[]{:S(2)}) collective-permute-start(bf16[256,1024]{1,0:T(8,128)(2,1)S(1)} %collective-permute-done), channel_id=1, source_target_pairs={{0,4},{4,8},{8,12},{12,16},{16,20},{20,24},{24,28},{28,0},{1,5},{5... | collective-permute-start | bytes 1572872 | tf_op jit(solution)/shard_map/ppermute | solution.py:13
  57.7 26.8 %collective-permute-start.2 = (bf16[256,1024]{1,0:T(8,128)(2,1)S(1)}, bf16[256,1024]{1,0:T(8,128)(2,1)S(1)}, u32[]{:S(2)}, u32[]{:S(2)}) collective-permute-start(bf16[256,1024]{1,0:T(8,128)(2,1)S(1)} %collective-permute-done.1), channel_id=1, source_target_pairs={{0,4},{4,8},{8,12},{12,16},{16,20},{20,24},{24,28},{28,0},{1,5},{5... | collective-permute-start | bytes 1572872 | tf_op jit(solution)/shard_map/ppermute | solution.py:13
  84.6 26.9 %collective-permute-start.3 = (bf16[256,1024]{1,0:T(8,128)(2,1)S(1)}, bf16[256,1024]{1,0:T(8,128)(2,1)S(1)}, u32[]{:S(2)}, u32[]{:S(2)}) collective-permute-start(bf16[256,1024]{1,0:T(8,128)(2,1)S(1)} %collective-permute-done.2), channel_id=1, source_target_pairs={{0,4},{4,8},{8,12},{12,16},{16,20},{20,24},{24,28},{28,0},{1,5},{5... | collective-permute-start | bytes 1572872 | tf_op jit(solution)/shard_map/ppermute | solution.py:13
  111.5 18.0 %collective-permute-start.4 = (bf16[256,1024]{1,0:T(8,128)(2,1)S(1)}, bf16[256,1024]{1,0:T(8,128)(2,1)S(1)}, u32[]{:S(2)}, u32[]{:S(2)}) collective-permute-start(bf16[256,1024]{1,0:T(8,128)(2,1)S(1)} %collective-permute-done.3), channel_id=1, source_target_pairs={{0,4},{4,8},{8,12},{12,16},{16,20},{20,24},{24,28},{28,0},{1,5},{5... | collective-permute-start | bytes 1572872 | tf_op jit(solution)/shard_map/ppermute | solution.py:13
  129.5 0.8 copy-start.1
  130.3 14.2 %collective-permute-start.5 = (bf16[256,1024]{1,0:T(8,128)(2,1)S(1)}, bf16[256,1024]{1,0:T(8,128)(2,1)}, u32[]{:S(2)}, u32[]{:S(2)}) collective-permute-start(bf16[256,1024]{1,0:T(8,128)(2,1)S(1)} %collective-permute-done.4), channel_id=1, source_target_pairs={{0,4},{4,8},{8,12},{12,16},{16,20},{20,24},{24,28},{28,0},{1,5},{5... | collective-permute-start | bytes 1572872 | tf_op jit(solution)/shard_map/ppermute | solution.py:13
  144.5 13.6 %collective-permute-start.6 = (bf16[256,1024]{1,0:T(8,128)(2,1)}, bf16[256,1024]{1,0:T(8,128)(2,1)}, u32[]{:S(2)}, u32[]{:S(2)}) collective-permute-start(bf16[256,1024]{1,0:T(8,128)(2,1)} %collective-permute-done.5), channel_id=1, source_target_pairs={{0,4},{4,8},{8,12},{12,16},{16,20},{20,24},{24,28},{28,0},{1,5},{5... | collective-permute-start | bytes 1572872 | tf_op jit(solution)/shard_map/ppermute | solution.py:13
  144.5 57.7 %all-to-all-start = ((bf16[4,1024,512]{2,1,0:T(8,128)(2,1)}), bf16[4,1024,512]{2,1,0:T(8,128)(2,1)}, u32[]{:S(2)}, u32[]{:S(2)}) async-start(bf16[4,1024,512]{2,1,0:T(8,128)(2,1)} %bitcast.8), calls=%async_computation | async-start | bytes 8388608 | tf_op jit(solution)/shard_map/all_to_all | solution.py:26
  149.5 119.4 %reduce-scatter.2.cloned.1.call-start = ((), (), s32[]{:S(2)}) async-start(), calls=%async_computation.4 | async-start | bytes 5242880 | tf_op jit(solution)/shard_map/reduce_scatter | solution.py:34
  149.6 14.3 %copy-start.2 = (bf16[256,1024]{1,0:T(8,128)(2,1)S(1)}, bf16[256,1024]{1,0:T(8,128)(2,1)}, u32[]{:S(2)}) copy-start(bf16[256,1024]{1,0:T(8,128)(2,1)} %copy-done.1) | copy-start | bytes 1572868
Sparse Core Ops, SparseCore 0:
  10.7 104.7 all-gather.4
  117.0 46.3 all-gather.2
  223.4 45.4 reduce-scatter.1
